TPU v7x, 32 devices: a whole 2x2x4 slice. The times are simulated.
32 devices in a mesh: sp: 8 (over z, x), tp: 4 (over y, core).
Axes of the slice: x: 2, y: 2, z: 4, core: 2. Of those that a mesh axis runs over, the one named last changes fastest.
Arguments:
- tokens: bfloat16 [4096, 4096], P(('sp', 'tp')), may hold values from -6 to 6
- lock_projector: bfloat16 [4096, 1024], P(None, 'tp'), may hold values from -0.01171875 to 0.01171875
- value_weight: bfloat16 [4096, 2048], P(None, 'tp'), may hold values from -0.0234375 to 0.0234375
- decay_weight: bfloat16 [4096, 1024], P(None, 'tp'), may hold values from -0.09375 to 0.09375
- decay_offset: float32 [1024], P('tp'), may hold values from -3.5 to 0
- fresh_question: bfloat16 [16, 64], P('tp'), may hold values from -6 to 6
Outputs:
- state_cache: bfloat16 [16, 64, 128], P('tp', 'sp')
- first_read: bfloat16 [16, 128], P('tp')
All inputs are finite; a program needn't handle non-finite values.
Results may differ from a plain program's by a relative error of at most 0.0034.
Values may be sent and summed in bfloat16 or wider, within the bound.
No kernel may reach another device: no remote copies, remote signals or barrier semaphores. Data moves between devices by JAX's collectives and lax.ppermute only.
A program may use at most 64 MiB of HBM per device.

v0:
```python
import math
import jax
import jax.numpy as jnp
from jax import lax
from jax.sharding import PartitionSpec as P

CUE_WIDTH = 64
DV = 128
decay_tau = 16.0


def carried_in(part, axis, combine, identity):
    count = lax.axis_size(axis)
    place = lax.axis_index(axis)
    ahead = count - 1 - place
    gathered = lax.all_gather(part, axis)
    state = jnp.zeros_like(part) + jnp.asarray(identity, part.dtype)

    def one(hop, state):
        source = count - 1 - hop
        return combine(state, lax.dynamic_index_in_dim(gathered, source, 0, False))

    return lax.fori_loop(0, ahead, one, state)


def add_logs(earlier, later_sum):
    return earlier + later_sum


def per_device(tokens, lock_projector, value_weight, decay_weight, decay_offset, fresh_question):
    key_cols = lock_projector.shape[1]
    value_cols = value_weight.shape[1]
    local_heads = key_cols // CUE_WIDTH
    combined = jnp.concatenate([lock_projector, value_weight, decay_weight], axis=1)
    projected = jnp.dot(
        lax.all_gather(tokens, "tp", axis=0, tiled=True),
        combined,
        preferred_element_type=jnp.float32,
    )
    span_rows = projected.shape[0]
    lock_vectors = projected[:, :key_cols].astype(jnp.bfloat16)
    value_rows = projected[:, key_cols : key_cols + value_cols].astype(jnp.bfloat16)
    decay_pre = projected[:, key_cols + value_cols :]
    length = span_rows * lax.axis_size("sp")
    log_decay = jax.nn.log_sigmoid(decay_pre + decay_offset[None, :] + math.log(length)) / decay_tau
    segment_overall = jnp.sum(log_decay, axis=0)
    later_total = carried_in(segment_overall, "sp", add_logs, jnp.zeros_like(segment_overall))
    after = (segment_overall + later_total)[None, :] - jnp.cumsum(log_decay, axis=0)
    weighted = (lock_vectors.astype(jnp.float32) * jnp.exp(after)).astype(jnp.bfloat16)
    lookup_probes = weighted.reshape(span_rows, local_heads, CUE_WIDTH)
    stored_contents = value_rows.reshape(span_rows, local_heads, DV)
    summands_list = jnp.einsum(
        "nyl,nyp->ylp", lookup_probes, stored_contents, preferred_element_type=jnp.float32
    )
    key_scale = CUE_WIDTH ** (-0.5)
    question_widened = fresh_question.astype(jnp.float32)
    row_span = CUE_WIDTH // lax.axis_size("sp")
    row_start = lax.axis_index("sp") * row_span
    recall_grid = lax.psum(summands_list, "sp")
    segment_lines = lax.dynamic_slice_in_dim(recall_grid, row_start, row_span, 1)
    attended_blend = key_scale * jnp.einsum(
        "qw,qwi->qi", question_widened, recall_grid, precision=lax.Precision.HIGHEST
    )
    state_cache = segment_lines.astype(jnp.bfloat16)
    first_read = attended_blend * lax.rsqrt(
        jnp.mean(attended_blend * attended_blend, axis=-1, keepdims=True) + 1.0
    )
    return (state_cache, first_read.astype(jnp.bfloat16))


def solution(mesh):
    in_specs = (
        P(("sp", "tp"), None),
        P(None, "tp"),
        P(None, "tp"),
        P(None, "tp"),
        P("tp"),
        P("tp", None),
    )
    out_specs = (P("tp", "sp", None), P("tp", None))
    return jax.shard_map(
        per_device, mesh=mesh, in_specs=in_specs, out_specs=out_specs, check_vma=False
    )
```

profile of v0, /device:TPU:0, one launch (start us, length us, event | category | flops | bytes accessed | tf_op | source)
XLA Modules:
  0.0 155.6 jit_solution(18224980167365922461)
XLA Ops:
  7.2 0.0 copy-start
  7.2 0.0 all-gather.4.cloned.1.call-start
  7.2 0.7 all-gather.4.cloned.1.call-update
  7.9 0.0 all-reduce.2.cloned.1.call-start
  8.0 0.0 copy-start.1
  8.0 38.8 %all-gather.4.cloned.1.call-done = bf16[512,4096]{1,0:T(8,128)(2,1)} async-done(((bf16[128,4096]{1,0:T(8,128)(2,1)}), bf16[512,4096]{1,0:T(8,128)(2,1)}) %all-gather.4.cloned.1.call-update) | async-done | bytes 4194320 | tf_op jit(solution)/shard_map/all_gather | solution.py:36
  46.8 8.3 %fusion.22 = (bf16[512,1024]{0,1:T(8,128)(2,1)S(1)}, f32[512,1024]{0,1:T(8,128)S(1)}) fusion(bf16[512,4096]{1,0:T(8,128)(2,1)} %all-gather.4.cloned.1.call-done, bf16[4096,256]{1,0:T(8,128)(2,1)} %param.11, bf16[4096,512]{1,0:T(8,128)(2,1)} %param.10, bf16[4096,256]{1,0:T(8,128)(2,1)} %param.9), kind=kOutput, calls=%fused_computation.31 | convolution fusion | flops 4320657408 | bytes 15728640 | tf_op jit(solution)/shard_map/dot_general | solution.py:35
  55.1 0.0 copy-done.1
  55.1 0.5 fusion.21
  55.6 20.5 %all-gather.1 = f32[8,1,256]{2,1,0:T(1,128)S(1)} all-gather(f32[1,1,256]{2,1,0:T(1,128)S(1)} %bitcast.54), channel_id=2, replica_groups=mesh['sp'=8,'tp'=4] {'sp'}, dimensions={0}, use_global_device_ids=true | all-gather | bytes 9216 | tf_op jit(solution)/shard_map/all_gather | solution.py:16
  76.1 0.3 while.12
  76.5 0.2 reshape.30
  76.7 0.2 copy.11
  76.9 0.1 fusion.23
  77.2 0.3 copy.12
  77.5 0.2 fusion.14
  77.6 1.0 fusion.24
  78.6 0.0 all-reduce.2.cloned.1.call-update
  78.6 67.0 %all-reduce.2.cloned.1.call-done = f32[4,64,128]{2,1,0:T(8,128)} async-done(((f32[4,64,128]{2,1,0:T(8,128)}), f32[4,64,128]{2,1,0:T(8,128)}) %all-reduce.2.cloned.1.call-update) | async-done | bytes 131088 | tf_op jit(solution)/shard_map/psum | solution.py:59
  145.6 0.0 copy-done
  145.6 1.1 fusion.17
  146.7 0.1 multiply_reduce_fusion
  146.8 0.6 multiply_convert_fusion
  147.5 1.3 dynamic-slice_convert_fusion
  (24 shorter events, 0.3 us)
Async XLA Ops:
  7.2 138.4 %copy-start = (bf16[4,64]{1,0:T(4,128)(2,1)S(1)}, bf16[4,64]{1,0:T(4,128)(2,1)}, u32[]{:S(2)}) copy-start(bf16[4,64]{1,0:T(4,128)(2,1)} %param.13) | copy-start | bytes 1540
  7.2 39.6 %all-gather.4.cloned.1.call-start = ((), (), s32[]{:S(2)}) async-start(), calls=%async_computation | async-start | bytes 5242880 | tf_op jit(solution)/shard_map/all_gather | solution.py:36
  7.9 137.7 %all-reduce.2.cloned.1.call-start = ((), (), s32[]{:S(2)}) async-start(), calls=%async_computation.1 | async-start | bytes 262144 | tf_op jit(solution)/shard_map/psum | solution.py:59
  8.0 47.1 %copy-start.1 = (f32[256]{0:T(256)S(1)}, f32[256]{0:T(256)}, u32[]{:S(2)}) copy-start(f32[256]{0:T(256)} %param.12) | copy-start | bytes 3076
Sparse Core Ops, SparseCore 0:
  9.5 37.1 all-gather.3
  78.7 66.8 all-reduce.1
where the time goes:
time: 156 us
  waiting for transfers between devices  106 us (68%)
  blocking collectives  20.5 us (13%)
  between operations  14.1 us (9%)
  matrix products  10.3 us (7%)
  local copies, waits for them, and re-layouts  2.13 us (1%)
  other arithmetic  1.74 us (1%)
    psum x1, waiting for transfers between devices, per_device(): recall_grid = lax.psum(summands_list, 'sp')  67 us
    all_gather x1, waiting for transfers between devices, per_device(): lax.all_gather(tokens, 'tp', axis=0, tiled=True)  38.8 us
    all_gather x1, blocking collectives, carried_in(): gathered = lax.all_gather(part, axis)  20.5 us
    dot_general x1, matrix products, per_device(): jnp.dot(lax.all_gather(tokens, 'tp', axis=0, tiled=True), combined, prefe...  8.32 us
  transfers between devices with their start and end apart: 2, of which 2 were waited for; matrix products, arithmetic and copies ran while one was open for 0% of the time, Pallas kernels for 0%

commit v1 on v0

--- a/solution.py
+++ b/solution.py
@@ -56,7 +56,8 @@
     question_widened = fresh_question.astype(jnp.float32)
     row_span = CUE_WIDTH // lax.axis_size("sp")
     row_start = lax.axis_index("sp") * row_span
-    recall_grid = lax.psum(summands_list, "sp")
+    parts = lax.all_gather(summands_list, "sp", axis=0, tiled=False)
+    recall_grid = parts.sum(axis=0)
     segment_lines = lax.dynamic_slice_in_dim(recall_grid, row_start, row_span, 1)
     attended_blend = key_scale * jnp.einsum(
         "qw,qwi->qi", question_widened, recall_grid, precision=lax.Precision.HIGHEST

time: 156 us -> 125 us (0.80)
  waiting for transfers between devices: 106 us -> 76.2 us
    psum x1 -> x0, waiting for transfers between devices: 67 us -> none  [per_device(): recall_grid = lax.psum(summands_list, 'sp')]
    all_gather x0 -> x1, waiting for transfers between devices: none -> 36.8 us  [per_device(): parts = lax.all_gather(summands_list, 'sp', axis=0, tiled=False)]
where the time goes in v1:
time: 125 us
  waiting for transfers between devices  76.2 us (61%)
  blocking collectives  20.5 us (16%)
  between operations  14.2 us (11%)
  matrix products  9.44 us (8%)
  other arithmetic  3.04 us (2%)
  local copies, waits for them, and re-layouts  1.42 us (1%)
    all_gather x1, waiting for transfers between devices, per_device(): lax.all_gather(tokens, 'tp', axis=0, tiled=True)  38.8 us
    all_gather x1, waiting for transfers between devices, per_device(): parts = lax.all_gather(summands_list, 'sp', axis=0, tiled=False)  36.8 us
    all_gather x1, blocking collectives, carried_in(): gathered = lax.all_gather(part, axis)  20.5 us
    dot_general x1, matrix products, per_device(): jnp.dot(lax.all_gather(tokens, 'tp', axis=0, tiled=True), combined, prefe...  8.32 us
  transfers between devices with their start and end apart: 2, of which 2 were waited for; matrix products, arithmetic and copies ran while one was open for 0% of the time, Pallas kernels for 0%

profile of v1, /device:TPU:0, one launch (start us, length us, event | category | flops | bytes accessed | tf_op | source)
XLA Modules:
  0.0 125.1 jit_solution(5661596509455975459)
XLA Ops:
  7.2 0.0 copy-start
  7.2 0.0 all-gather.6.cloned.1.call-start
  7.2 0.7 all-gather.6.cloned.1.call-update
  7.9 0.0 all-gather.8.cloned.1.call-start
  8.0 0.0 copy-start.1
  8.0 38.8 %all-gather.6.cloned.1.call-done = bf16[512,4096]{1,0:T(8,128)(2,1)} async-done(((bf16[128,4096]{1,0:T(8,128)(2,1)}), bf16[512,4096]{1,0:T(8,128)(2,1)}) %all-gather.6.cloned.1.call-update) | async-done | bytes 4194320 | tf_op jit(solution)/shard_map/all_gather | solution.py:36
  46.8 8.3 %fusion.22 = (bf16[512,1024]{0,1:T(8,128)(2,1)S(1)}, f32[512,1024]{0,1:T(8,128)S(1)}) fusion(bf16[512,4096]{1,0:T(8,128)(2,1)} %all-gather.6.cloned.1.call-done, bf16[4096,256]{1,0:T(8,128)(2,1)} %param.11, bf16[4096,512]{1,0:T(8,128)(2,1)} %param.10, bf16[4096,256]{1,0:T(8,128)(2,1)} %param.9), kind=kOutput, calls=%fused_computation.31 | convolution fusion | flops 4320657408 | bytes 15728640 | tf_op jit(solution)/shard_map/dot_general | solution.py:35
  55.1 0.0 copy-done.1
  55.1 0.5 fusion.21
  55.6 20.5 %all-gather.2 = f32[8,1,256]{2,1,0:T(1,128)S(1)} all-gather(f32[1,1,256]{2,1,0:T(1,128)S(1)} %bitcast.56), channel_id=2, replica_groups=mesh['sp'=8,'tp'=4] {'sp'}, dimensions={0}, use_global_device_ids=true | all-gather | bytes 9216 | tf_op jit(solution)/shard_map/all_gather | solution.py:16
  76.1 0.3 while.12
  76.5 0.2 reshape.30
  76.7 0.3 copy.11
  76.9 0.1 fusion.23
  77.2 0.3 copy.12
  77.5 0.2 fusion.14
  77.6 0.9 fusion.24
  78.6 0.0 all-gather.8.cloned.1.call-update
  78.6 36.8 %all-gather.8.cloned.1.call-done = f32[32,64,128]{2,1,0:T(8,128)} async-done(((f32[4,64,128]{2,1,0:T(8,128)}), f32[32,64,128]{2,1,0:T(8,128)}) %all-gather.8.cloned.1.call-update) | async-done | bytes 1048592 | tf_op jit(solution)/shard_map/all_gather | solution.py:59
  115.4 1.3 %reduce_sum.28 = f32[4,64,128]{2,1,0:T(8,128)S(1)} reduce(f32[8,4,64,128]{3,2,1,0:T(8,128)} %bitcast.50, f32[]{:T(128)} %constant.48.clone.1), dimensions={0}, to_apply=%region_5.6 | reduce | flops 229376 | bytes 1179652 | tf_op jit(solution)/shard_map/reduce_sum | solution.py:60
  116.7 0.0 copy-done
  116.7 0.2 fusion.17
  116.9 0.1 multiply_reduce_fusion
  117.0 0.6 multiply_convert_fusion
  117.6 0.6 dynamic-slice_convert_fusion
  (24 shorter events, 0.3 us)
Async XLA Ops:
  7.2 109.5 %copy-start = (bf16[4,64]{1,0:T(4,128)(2,1)S(1)}, bf16[4,64]{1,0:T(4,128)(2,1)}, u32[]{:S(2)}) copy-start(bf16[4,64]{1,0:T(4,128)(2,1)} %param.13) | copy-start | bytes 1540
  7.2 39.6 %all-gather.6.cloned.1.call-start = ((), (), s32[]{:S(2)}) async-start(), calls=%async_computation | async-start | bytes 5242880 | tf_op jit(solution)/shard_map/all_gather | solution.py:36
  7.9 107.5 %all-gather.8.cloned.1.call-start = ((), (), s32[]{:S(2)}) async-start(), calls=%async_computation.1 | async-start | bytes 1179648 | tf_op jit(solution)/shard_map/all_gather | solution.py:59
  8.0 47.1 %copy-start.1 = (f32[256]{0:T(256)S(1)}, f32[256]{0:T(256)}, u32[]{:S(2)}) copy-start(f32[256]{0:T(256)} %param.12) | copy-start | bytes 3076
Sparse Core Ops, SparseCore 0:
  9.5 37.1 all-gather.5
  78.7 36.5 all-gather.7
